TPU v7x, 32 devices: a whole 2x2x4 slice. The times are simulated.
32 devices in a mesh: ep: 8 (over z, y), tp: 4 (over x, core).
Axes of the slice: x: 2, y: 2, z: 4, core: 2. Of those that a mesh axis runs over, the one named last changes fastest.
Arguments:
- tokens: bfloat16 [128, 1024], P('ep'), may hold values from -6 to 6
- attn_gain: float32 [1024], replicated, may hold values from 0.1 to 1.9
- q_down: bfloat16 [1024, 512], P(None, 'tp'), may hold values from -0.1875 to 0.1875
- kv_down: bfloat16 [1024, 512], P(None, 'tp'), may hold values from -0.1875 to 0.1875
- rope_down: bfloat16 [1024, 32], replicated, may hold values from -0.1875 to 0.1875
- q_latent_gain: float32 [512], replicated, may hold values from 0.1 to 1.9
- kv_latent_gain: float32 [512], replicated, may hold values from 0.1 to 1.9
- q_up: bfloat16 [512, 768], P(None, 'tp'), may hold values from -0.25 to 0.25
- query_gain: float32 [8, 96], P('tp'), may hold values from 0.4 to 48
- key_up: bfloat16 [512, 512], P(None, 'tp'), may hold values from -0.25 to 0.25
- value_up: bfloat16 [512, 512], P(None, 'tp'), may hold values from -0.25 to 0.25
- attn_out: bfloat16 [512, 1024], P('tp'), may hold values from -0.25 to 0.25
- cache_latent: bfloat16 [128, 512, 512], P(('ep', 'tp')), may hold values from -6 to 6
- cache_rope: bfloat16 [128, 32, 512], P(('ep', 'tp')), may hold values from -6 to 6
- lengths: int32 [128], P('ep'), may hold values from 1 to 512, as said below
- moe_gain: float32 [1024], replicated, may hold values from 0.1 to 1.9
- route: int32 [128, 6], P('ep'), may hold values from 0 to 7, as said below
- route_weight: float32 [128, 6], P('ep'), may hold values from 0.1 to 1
- expert_gate: bfloat16 [8, 1024, 512], P('ep', None, 'tp'), may hold values from -0.1875 to 0.1875
- expert_up: bfloat16 [8, 1024, 512], P('ep', None, 'tp'), may hold values from -0.1875 to 0.1875
- expert_down: bfloat16 [8, 512, 1024], P('ep', 'tp'), may hold values from -0.25 to 0.25
Outputs:
- mixed_out: bfloat16 [128, 1024], P('ep', 'tp')
- new_latent: bfloat16 [128, 512], P('ep', 'tp')
- new_rope: bfloat16 [128, 32], P('ep')
Inputs may be any that keep to these rules, and one draw needn't show every extreme that they name: `route`: each row names 6 different experts that lie in one group of 8 consecutive expert numbers. Among the rows of the 16 sequences of one index of ep no expert is named more than 12 times, and some expert is named exactly 12 times by the rows of every index of ep. `lengths`: some sequence has exactly 512 cached positions.
All inputs are finite; a program needn't handle non-finite values.
Results may differ from a plain program's by a relative error of at most 0.02.
Values may be sent and summed in bfloat16 or wider, within the bound.
A program may use at most 64 MiB of HBM per device.

v0:
```python
import jax
import jax.numpy as jnp
from jax import lax
from jax.sharding import PartitionSpec as P

NOPE = 64
VDIM = 64
QK = 96
EPG = 8
EPS = 1e-06
ROPE_BASE = 10000.0


def rms_scaled(values_in, gain_vec):
    values_in = values_in.astype(jnp.float32)
    return (
        values_in
        * lax.rsqrt(jnp.mean(values_in * values_in, axis=-1, keepdims=True) + EPS)
        * gain_vec
    )


def rotate_last(values_in, positions):
    half_dim = values_in.shape[-1] // 2
    inverse = ROPE_BASE ** (-jnp.arange(half_dim, dtype=jnp.float32) / half_dim)
    angles = positions.astype(jnp.float32)[..., None] * inverse
    lower_half = values_in[..., :half_dim]
    upper_half = values_in[..., half_dim:]
    return jnp.concatenate(
        [
            lower_half * jnp.cos(angles) - upper_half * jnp.sin(angles),
            upper_half * jnp.cos(angles) + lower_half * jnp.sin(angles),
        ],
        -1,
    )


def rotate_rows(values_in, positions):
    half_dim = values_in.shape[1] // 2
    inverse = ROPE_BASE ** (-jnp.arange(half_dim, dtype=jnp.float32) / half_dim)
    angles = inverse[:, None] * positions.astype(jnp.float32)[None, :]
    lower_half = values_in[:, :half_dim]
    upper_half = values_in[:, half_dim:]
    return jnp.concatenate(
        [
            lower_half * jnp.cos(angles) - upper_half * jnp.sin(angles),
            upper_half * jnp.cos(angles) + lower_half * jnp.sin(angles),
        ],
        1,
    )


def shards(
    tokens,
    attn_gain,
    q_down,
    kv_down,
    rope_down,
    q_latent_gain,
    kv_latent_gain,
    q_up,
    query_gain,
    key_up,
    value_up,
    attn_out,
    cache_latent,
    cache_rope,
    lengths,
    moe_gain,
    route,
    route_weight,
    expert_gate,
    expert_up,
    expert_down,
):
    score_scale = QK ** (-0.5)
    tp_count = lax.axis_size("tp")
    tp_index = lax.axis_index("tp")
    normed = rms_scaled(tokens, attn_gain).astype(jnp.bfloat16)
    q_part = jnp.dot(normed, q_down, preferred_element_type=jnp.float32).astype(jnp.bfloat16)
    kv_part = jnp.dot(normed, kv_down, preferred_element_type=jnp.float32).astype(jnp.bfloat16)
    q_raw, kv_raw = (
        lax.all_gather(q_part, "tp", axis=1, tiled=True),
        lax.all_gather(kv_part, "tp", axis=1, tiled=True),
    )
    new_rope = jnp.dot(normed, rope_down, preferred_element_type=jnp.float32).astype(jnp.bfloat16)
    q_lat = rms_scaled(q_raw, q_latent_gain).astype(jnp.bfloat16)
    latent_new = rms_scaled(kv_raw, kv_latent_gain).astype(jnp.bfloat16)
    kv_cols = kv_part.shape[1]
    new_latent = lax.dynamic_slice_in_dim(latent_new, tp_index * kv_cols, kv_cols, 1)
    heads_here = query_gain.shape[0]
    seq_count = tokens.shape[0]
    query_head = rms_scaled(
        jnp.dot(q_lat, q_up, preferred_element_type=jnp.float32).reshape(seq_count, heads_here, QK),
        query_gain,
    )
    query_head = jnp.concatenate(
        [query_head[..., :NOPE], rotate_last(query_head[..., NOPE:], lengths[:, None])], -1
    ).astype(jnp.bfloat16)
    absorbed = jnp.einsum(
        "shn,rhn->shr",
        query_head[..., :NOPE],
        key_up.reshape(-1, heads_here, NOPE),
        preferred_element_type=jnp.float32,
    ).astype(jnp.bfloat16)
    rot_query = query_head[..., NOPE:]
    absorbed_mine, rot_mine = (
        lax.all_to_all(absorbed, "tp", split_axis=0, concat_axis=1, tiled=True),
        lax.all_to_all(rot_query, "tp", split_axis=0, concat_axis=1, tiled=True),
    )
    seqs_mine = cache_latent.shape[0]
    first_seq = tp_index * seqs_mine
    len_mine = lax.dynamic_slice_in_dim(lengths, first_seq, seqs_mine, 0)
    latent_mine = lax.dynamic_slice_in_dim(latent_new, first_seq, seqs_mine, 0)
    key_new = rotate_last(
        lax.dynamic_slice_in_dim(new_rope, first_seq, seqs_mine, 0).astype(jnp.float32), len_mine
    ).astype(jnp.bfloat16)
    positions = jnp.arange(cache_latent.shape[1], dtype=jnp.int32)
    rotated_keys = rotate_rows(cache_rope.astype(jnp.float32), positions).astype(jnp.bfloat16)
    scores = (
        jnp.einsum("shr,sjr->shj", absorbed_mine, cache_latent, preferred_element_type=jnp.float32)
        + jnp.einsum("shp,spj->shj", rot_mine, rotated_keys, preferred_element_type=jnp.float32)
    ) * score_scale
    self_score = (
        jnp.einsum("shr,sr->sh", absorbed_mine, latent_mine, preferred_element_type=jnp.float32)
        + jnp.einsum("shp,sp->sh", rot_mine, key_new, preferred_element_type=jnp.float32)
    ) * score_scale
    valid_keys = positions[None, :] < len_mine[:, None]
    masked = jnp.where(valid_keys[:, None, :], scores, -jnp.inf)
    row_max = jnp.maximum(jnp.max(masked, axis=-1), self_score)
    weights = jnp.exp(masked - row_max[..., None])
    self_weight = jnp.exp(self_score - row_max)
    total_weight = jnp.sum(weights, axis=-1) + self_weight
    latent_sum = jnp.einsum(
        "shj,sjr->shr",
        weights.astype(jnp.bfloat16),
        cache_latent,
        preferred_element_type=jnp.float32,
    )
    latent_sum = (
        latent_sum
        + self_weight.astype(jnp.bfloat16).astype(jnp.float32)[..., None]
        * latent_mine.astype(jnp.float32)[:, None, :]
    )
    attended = (latent_sum / total_weight[..., None]).astype(jnp.bfloat16)
    attended_heads = lax.all_to_all(attended, "tp", split_axis=1, concat_axis=0, tiled=True)
    head_values = (
        jnp.einsum(
            "shr,rhv->shv",
            attended_heads,
            value_up.reshape(-1, heads_here, VDIM),
            preferred_element_type=jnp.float32,
        )
        .astype(jnp.bfloat16)
        .reshape(seq_count, heads_here * VDIM)
    )
    head_sum = lax.psum(
        jnp.dot(head_values, attn_out, preferred_element_type=jnp.float32).astype(jnp.bfloat16),
        "tp",
    ).astype(jnp.float32)
    attn_resid = (tokens.astype(jnp.float32) + head_sum).astype(jnp.bfloat16)
    moe_input = rms_scaled(attn_resid, moe_gain).astype(jnp.bfloat16)
    topk_here = route.shape[1]
    experts_all = expert_gate.shape[0] * lax.axis_size("ep")
    group_cap = min(seq_count, max(2, 2 * seq_count * EPG // experts_all))
    capacity = (topk_here * group_cap + EPG - 1) // EPG
    flat_route = route.reshape(-1)
    row_order = jnp.arange(flat_route.shape[0])
    slot_rank = jnp.sum(
        (flat_route[:, None] == flat_route[None, :]) & (row_order[None, :] < row_order[:, None]),
        axis=1,
    )
    slot_index = flat_route * capacity + slot_rank
    model_width = tokens.shape[1]
    quarter_cols = model_width // tp_count
    residual = lax.dynamic_slice_in_dim(attn_resid, tp_index * quarter_cols, quarter_cols, 1)
    own_cols = lax.dynamic_slice_in_dim(moe_input, tp_index * quarter_cols, quarter_cols, 1)
    buffer = jnp.zeros((experts_all * capacity, own_cols.shape[1]), jnp.bfloat16)
    buffer = buffer.at[slot_index].set(jnp.repeat(own_cols, topk_here, axis=0))
    arrived = lax.all_to_all(
        buffer.reshape(experts_all, capacity, own_cols.shape[1]),
        "ep",
        split_axis=0,
        concat_axis=1,
        tiled=True,
    )
    piece = lax.all_gather(arrived, "tp", axis=2, tiled=True)
    gate_pre = jnp.einsum("erd,edf->erf", piece, expert_gate, preferred_element_type=jnp.float32)
    up_pre = jnp.einsum("erd,edf->erf", piece, expert_up, preferred_element_type=jnp.float32)
    hidden = (jax.nn.silu(gate_pre) * up_pre).astype(jnp.bfloat16)
    partial_value = jnp.einsum(
        "erf,efd->erd", hidden, expert_down, preferred_element_type=jnp.float32
    )
    reduced = lax.psum_scatter(
        partial_value.astype(jnp.bfloat16), "tp", scatter_dimension=2, tiled=True
    )
    returned = lax.all_to_all(reduced, "ep", split_axis=1, concat_axis=0, tiled=True)
    picked = (
        returned.reshape(-1, quarter_cols)[slot_index]
        .astype(jnp.float32)
        .reshape(seq_count, topk_here, quarter_cols)
    )
    mixed_out = (
        residual.astype(jnp.float32) + jnp.sum(picked * route_weight[..., None], axis=1)
    ).astype(jnp.bfloat16)
    return (mixed_out, new_latent, new_rope)


def solution(mesh):
    placed = (
        P("ep", None),
        P(),
        P(None, "tp"),
        P(None, "tp"),
        P(),
        P(),
        P(),
        P(None, "tp"),
        P("tp", None),
        P(None, "tp"),
        P(None, "tp"),
        P("tp", None),
        P(("ep", "tp"), None, None),
        P(("ep", "tp"), None, None),
        P("ep"),
        P(),
        P("ep", None),
        P("ep", None),
        P("ep", None, "tp"),
        P("ep", None, "tp"),
        P("ep", "tp", None),
    )
    return jax.shard_map(
        shards,
        mesh=mesh,
        in_specs=placed,
        out_specs=(P("ep", "tp"), P("ep", "tp"), P("ep", None)),
        check_vma=False,
    )
```

profile of v0, /device:TPU:0, one launch (start us, length us, event | category | flops | bytes accessed | tf_op | source)
XLA Modules:
  0.0 125.3 jit_solution(8537989430489213607)
XLA Ops:
  7.2 1.0 fusion.19
  8.3 1.2 convolution_convert_fusion.6
  9.5 6.1 %all_gather.9 = bf16[16,512]{1,0:T(8,128)(2,1)S(1)} all-gather(bf16[16,128]{1,0:T(8,128)(2,1)S(1)} %convolution_convert_fusion.6), channel_id=1, replica_groups=mesh['ep'=8,'tp'=4] {'tp'}, dimensions={1}, use_global_device_ids=true | all-gather | bytes 20480 | tf_op jit(solution)/shard_map/all_gather | solution.py:83
  15.7 1.1 fusion.42
  17.1 0.7 convert_element_type.132
  17.8 0.8 fusion.46
  18.9 0.7 reshape.330
  19.5 3.3 %all-to-all-start.1 = ((bf16[4,2,128]{2,1,0:T(2,128)(2,1)}), bf16[4,2,128]{2,1,0:T(2,128)(2,1)S(1)}, u32[]{:S(2)}, u32[]{:S(2)}) async-start(bf16[4,2,128]{2,1,0:T(2,128)(2,1)} %reshape.330), calls=%async_computation.1 | async-start | bytes 4096 | tf_op jit(solution)/shard_map/all_to_all | solution.py:109
  22.8 0.7 broadcast_multiply_fusion
  23.5 0.8 copy.100
  24.3 0.2 convert_reduce_fusion
  24.5 1.0 copy.90
  25.7 0.9 convert_element_type.133
  26.6 0.2 multiply_cosine_fusion
  26.8 0.7 fusion.71
  27.6 1.2 convolution_convert_fusion.5
  28.8 5.4 %all_gather.10 = bf16[16,512]{1,0:T(8,128)(2,1)S(1)} all-gather(bf16[16,128]{1,0:T(8,128)(2,1)S(1)} %convolution_convert_fusion.5), channel_id=1, replica_groups=mesh['ep'=8,'tp'=4] {'tp'}, dimensions={1}, use_global_device_ids=true | all-gather | bytes 20480 | tf_op jit(solution)/shard_map/all_gather | solution.py:84
  34.5 0.2 convolution_convert_fusion.4
  35.1 0.6 copy.91
  35.7 3.3 %all-to-all-start = ((bf16[16,2,512]{2,1,0:T(2,128)(2,1)}), bf16[16,2,512]{2,1,0:T(2,128)(2,1)S(1)}, u32[]{:S(2)}, u32[]{:S(2)}) async-start(bf16[16,2,512]{2,1,0:T(2,128)(2,1)} %copy.91), calls=%async_computation | async-start | bytes 65536 | tf_op jit(solution)/shard_map/all_to_all | solution.py:108
  39.2 3.7 %all-to-all-done = bf16[16,2,512]{2,1,0:T(2,128)(2,1)S(1)} async-done(((bf16[16,2,512]{2,1,0:T(2,128)(2,1)}), bf16[16,2,512]{2,1,0:T(2,128)(2,1)S(1)}, u32[]{:S(2)}, u32[]{:S(2)}) %all-to-all-start) | async-done | bytes 32800 | tf_op jit(solution)/shard_map/all_to_all | solution.py:108
  43.0 0.6 fusion.73
  43.6 0.1 fusion.49
  43.8 0.2 fusion.72
  44.0 0.2 fusion.23
  44.2 0.4 fusion.4
  44.7 0.6 copy.95
  45.3 3.3 %all-to-all-start.2 = ((bf16[4,8,512]{2,0,1:T(4,128)(2,1)}), bf16[4,8,512]{2,0,1:T(4,128)(2,1)S(1)}, u32[]{:S(2)}, u32[]{:S(2)}) async-start(bf16[4,8,512]{2,0,1:T(4,128)(2,1)} %copy.95), calls=%async_computation.2 | async-start | bytes 65536 | tf_op jit(solution)/shard_map/all_to_all | solution.py:146
  48.7 0.8 dynamic-slice
  49.5 2.9 %all-to-all-done.2 = bf16[4,8,512]{2,0,1:T(4,128)(2,1)S(1)} async-done(((bf16[4,8,512]{2,0,1:T(4,128)(2,1)}), bf16[4,8,512]{2,0,1:T(4,128)(2,1)S(1)}, u32[]{:S(2)}, u32[]{:S(2)}) %all-to-all-start.2) | async-done | bytes 32800 | tf_op jit(solution)/shard_map/all_to_all | solution.py:146
  52.5 0.1 fusion.7
  52.8 0.1 convolution_convert_fusion.1
  52.9 10.3 %psum.7 = bf16[16,1024]{1,0:T(8,128)(2,1)S(1)} all-reduce(bf16[16,1024]{1,0:T(8,128)(2,1)S(1)} %convolution_convert_fusion.1), channel_id=1, replica_groups=mesh['ep'=8,'tp'=4] {'tp'}, use_global_device_ids=true, to_apply=%region_6.7 | all-reduce | flops 16384 | bytes 65536 | tf_op jit(solution)/shard_map/psum | solution.py:157
  63.4 0.9 scatter_custom_fusion
  64.4 12.8 %all_to_all.75 = bf16[8,12,256]{2,1,0:T(8,128)(2,1)S(1)} all-to-all(bf16[8,12,256]{2,1,0:T(8,128)(2,1)S(1)} %reshape.301), channel_id=1, replica_groups=mesh['ep'=8,'tp'=4] {'ep'}, dimensions={0} | all-to-all | bytes 98304 | tf_op jit(solution)/shard_map/all_to_all | solution.py:180
  77.2 5.6 %all_gather.11 = bf16[1,96,1024]{2,1,0:T(8,128)(2,1)S(1)} all-gather(bf16[1,96,256]{2,1,0:T(8,128)(2,1)S(1)} %all_to_all.68), channel_id=1, replica_groups=mesh['ep'=8,'tp'=4] {'tp'}, dimensions={2}, use_global_device_ids=true | all-gather | bytes 245760 | tf_op jit(solution)/shard_map/all_gather | solution.py:187
  82.8 0.2 fusion.11
  83.1 1.0 fusion
  84.2 17.4 %reduce-scatter.2.cloned.1.call-done = bf16[1,96,256]{2,1,0:T(8,128)(2,1)} async-done(((bf16[1,96,1024]{2,1,0:T(8,128)(2,1)}), bf16[1,96,256]{2,1,0:T(8,128)(2,1)}) %reduce-scatter.2.cloned.1.call-update) | async-done | bytes 49168 | tf_op jit(solution)/shard_map/reduce_scatter | solution.py:194
  101.6 0.9 copy.122
  102.5 0.5 broadcast.235
  103.0 0.9 reduce
  103.9 0.6 reshape.332
  104.6 5.5 %all-to-all-start.4 = ((bf16[8,2,1536]{2,1,0:T(2,128)(2,1)}), bf16[8,2,1536]{2,1,0:T(2,128)(2,1)S(1)}, u32[]{:S(2)}, u32[]{:S(2)}) async-start(bf16[8,2,1536]{2,1,0:T(2,128)(2,1)} %reshape.332), calls=%async_computation.5 | async-start | bytes 98304 | tf_op jit(solution)/shard_map/all_to_all | solution.py:197
  110.1 0.6 constant_dynamic-slice_fusion
  110.7 6.2 %all-to-all-done.4 = bf16[8,2,1536]{2,1,0:T(2,128)(2,1)S(1)} async-done(((bf16[8,2,1536]{2,1,0:T(2,128)(2,1)}), bf16[8,2,1536]{2,1,0:T(2,128)(2,1)S(1)}, u32[]{:S(2)}, u32[]{:S(2)}) %all-to-all-start.4) | async-done | bytes 49184 | tf_op jit(solution)/shard_map/all_to_all | solution.py:197
  116.9 0.8 gather_fusion
  117.8 0.6 add_convert_fusion.1
  (80 shorter events, 2.8 us)
Async XLA Ops:
  7.2 35.8 %copy-start = (bf16[4,512,512]{2,1,0:T(8,128)(2,1)S(1)}, bf16[4,512,512]{2,1,0:T(8,128)(2,1)}, u32[]{:S(2)}) copy-start(bf16[4,512,512]{2,1,0:T(8,128)(2,1)} %param.33) | copy-start | bytes 6291460
  7.2 27.3 %copy-start.5 = (bf16[16,1024]{1,0:T(8,128)(2,1)S(1)}, bf16[16,1024]{1,0:T(8,128)(2,1)}, u32[]{:S(2)}) copy-start(bf16[16,1024]{1,0:T(8,128)(2,1)} %param.21) | copy-start | bytes 98308
  7.2 27.3 %copy-start.11 = (f32[1024]{0:T(1024)S(1)}, f32[1024]{0:T(1024)}, u32[]{:S(2)}) copy-start(f32[1024]{0:T(1024)} %param.22) | copy-start | bytes 12292
  7.2 27.1 %copy-start.8 = (f32[512]{0:T(512)S(1)}, f32[512]{0:T(512)}, u32[]{:S(2)}) copy-start(f32[512]{0:T(512)} %param.27) | copy-start | bytes 6148
  7.2 27.2 %copy-start.10 = (bf16[1024,32]{0,1:T(8,128)(2,1)S(1)}, bf16[1024,32]{0,1:T(8,128)(2,1)}, u32[]{:S(2)}) copy-start(bf16[1024,32]{0,1:T(8,128)(2,1)} %param.25) | copy-start | bytes 196612
  19.5 16.2 %all-to-all-start.1 = ((bf16[4,2,128]{2,1,0:T(2,128)(2,1)}), bf16[4,2,128]{2,1,0:T(2,128)(2,1)S(1)}, u32[]{:S(2)}, u32[]{:S(2)}) async-start(bf16[4,2,128]{2,1,0:T(2,128)(2,1)} %reshape.330), calls=%async_computation.1 | async-start | bytes 4096 | tf_op jit(solution)/shard_map/all_to_all | solution.py:109
  34.7 10.0 %copy-start.9 = (bf16[16,32]{1,0:T(8,128)(2,1)}, bf16[16,32]{1,0:T(8,128)(2,1)S(1)}, u32[]{:S(2)}) copy-start(bf16[16,32]{1,0:T(8,128)(2,1)S(1)} %convolution_convert_fusion.4) | copy-start | bytes 3076
  35.7 7.2 %all-to-all-start = ((bf16[16,2,512]{2,1,0:T(2,128)(2,1)}), bf16[16,2,512]{2,1,0:T(2,128)(2,1)S(1)}, u32[]{:S(2)}, u32[]{:S(2)}) async-start(bf16[16,2,512]{2,1,0:T(2,128)(2,1)} %copy.91), calls=%async_computation | async-start | bytes 65536 | tf_op jit(solution)/shard_map/all_to_all | solution.py:108
  43.0 5.6 %copy-start.6 = (bf16[512,128]{1,0:T(8,128)(2,1)S(1)}, bf16[512,128]{1,0:T(8,128)(2,1)}, u32[]{:S(2)}) copy-start(bf16[512,128]{1,0:T(8,128)(2,1)} %param.31) | copy-start | bytes 393220
  43.6 9.1 %copy-start.1 = (bf16[128,1024]{1,0:T(8,128)(2,1)S(1)}, bf16[128,1024]{1,0:T(8,128)(2,1)}, u32[]{:S(2)}) copy-start(bf16[128,1024]{1,0:T(8,128)(2,1)} %param.32) | copy-start | bytes 786436
  44.2 38.6 %copy-start.2 = (bf16[1,1024,128]{2,1,0:T(8,128)(2,1)S(1)}, bf16[1,1024,128]{2,1,0:T(8,128)(2,1)}, u32[]{:S(2)}) copy-start(bf16[1,1024,128]{2,1,0:T(8,128)(2,1)} %param.39) | copy-start | bytes 786436
  44.2 38.8 %copy-start.3 = (bf16[1,128,1024]{2,1,0:T(8,128)(2,1)S(1)}, bf16[1,128,1024]{2,1,0:T(8,128)(2,1)}, u32[]{:S(2)}) copy-start(bf16[1,128,1024]{2,1,0:T(8,128)(2,1)} %param.41) | copy-start | bytes 786436
  44.2 38.8 %copy-start.4 = (bf16[1,1024,128]{2,1,0:T(8,128)(2,1)S(1)}, bf16[1,1024,128]{2,1,0:T(8,128)(2,1)}, u32[]{:S(2)}) copy-start(bf16[1,1024,128]{2,1,0:T(8,128)(2,1)} %param.40) | copy-start | bytes 786436
  44.7 39.5 %copy-start.7 = (f32[16,6]{0,1:T(8,128)S(1)}, f32[16,6]{0,1:T(8,128)}, u32[]{:S(2)}) copy-start(f32[16,6]{0,1:T(8,128)} %param.38) | copy-start | bytes 1156
  45.3 7.2 %all-to-all-start.2 = ((bf16[4,8,512]{2,0,1:T(4,128)(2,1)}), bf16[4,8,512]{2,0,1:T(4,128)(2,1)S(1)}, u32[]{:S(2)}, u32[]{:S(2)}) async-start(bf16[4,8,512]{2,0,1:T(4,128)(2,1)} %copy.95), calls=%async_computation.2 | async-start | bytes 65536 | tf_op jit(solution)/shard_map/all_to_all | solution.py:146
  48.6 53.1 %reduce-scatter.2.cloned.1.call-start = ((), (), s32[]{:S(2)}) async-start(), calls=%async_computation.6 | async-start | bytes 245760 | tf_op jit(solution)/shard_map/reduce_scatter | solution.py:194
  104.6 12.3 %all-to-all-start.4 = ((bf16[8,2,1536]{2,1,0:T(2,128)(2,1)}), bf16[8,2,1536]{2,1,0:T(2,128)(2,1)S(1)}, u32[]{:S(2)}, u32[]{:S(2)}) async-start(bf16[8,2,1536]{2,1,0:T(2,128)(2,1)} %reshape.332), calls=%async_computation.5 | async-start | bytes 98304 | tf_op jit(solution)/shard_map/all_to_all | solution.py:197
Sparse Core Ops, SparseCore 0:
  84.2 17.3 reduce-scatter.1
where the time goes:
time: 126 us; the launch traced here: 125 us
  blocking collectives  40.2 us (32%)
  waiting for transfers between devices  30.3 us (24%)
  starting transfers between devices  15.3 us (12%)
  between operations  14.4 us (11%)
  local copies, waits for them, and re-layouts  9.87 us (8%)
  other arithmetic  8.27 us (7%)
  matrix products  6.88 us (5%)
    reduce_scatter x1, waiting for transfers between devices, shards(): lax.psum_scatter(partial_value.astype(jnp.bfloat16), 'tp', scatter_dimens...  17.4 us
    all_to_all x1, blocking collectives, shards(): lax.all_to_all(buffer.reshape(experts_all, capacity, own_cols.shape[1]),...  12.8 us
    psum x1, blocking collectives, shards(): lax.psum(jnp.dot(head_values, attn_out, preferred_element_type=jnp.float3...  10.3 us
    all_to_all x1, waiting for transfers between devices, shards(): lax.all_to_all(reduced, 'ep', split_axis=1, concat_axis=0, tiled=True)  6.2 us
    all_gather x1, blocking collectives, shards(): lax.all_gather(q_part, 'tp', axis=1, tiled=True)  6.14 us
    all_gather x1, blocking collectives, shards(): piece = lax.all_gather(arrived, 'tp', axis=2, tiled=True)  5.6 us
    all_to_all x1, starting transfers between devices, shards(): lax.all_to_all(reduced, 'ep', split_axis=1, concat_axis=0, tiled=True)  5.52 us
    all_gather x1, blocking collectives, shards(): lax.all_gather(kv_part, 'tp', axis=1, tiled=True)  5.42 us
  transfers between devices with their start and end apart: 5, of which 4 were waited for; matrix products, arithmetic and copies ran while one was open for 7% of the time, Pallas kernels for 0%

commit v1 on v0

--- a/solution.py
+++ b/solution.py
@@ -154,9 +154,12 @@
         .astype(jnp.bfloat16)
         .reshape(seq_count, heads_here * VDIM)
     )
-    head_sum = lax.psum(
-        jnp.dot(head_values, attn_out, preferred_element_type=jnp.float32).astype(jnp.bfloat16),
-        "tp",
+    head_sum = jnp.sum(
+        lax.all_gather(
+            jnp.dot(head_values, attn_out, preferred_element_type=jnp.float32).astype(jnp.bfloat16),
+            "tp",
+        ),
+        axis=0,
     ).astype(jnp.float32)
     attn_resid = (tokens.astype(jnp.float32) + head_sum).astype(jnp.bfloat16)
     moe_input = rms_scaled(attn_resid, moe_gain).astype(jnp.bfloat16)

time: 126 us -> 120 us (0.952)
  blocking collectives: 40.2 us -> 35.4 us
    psum x1 -> x0, blocking collectives: 10.3 us -> none  [shards(): lax.psum(jnp.dot(head_values, attn_out, preferred_element_type=jnp.float3...]
    all_gather x0 -> x1, blocking collectives: none -> 5.41 us  [shards(): lax.all_gather(jnp.dot(head_values, attn_out, preferred_element_type=jnp....]
  transfers between devices with their start and end apart: 5 -> 5, of which waited for: 4 -> 4; matrix products, arithmetic and copies ran while one was open for 7% -> 8% of each run, Pallas kernels for 0% -> 0%
where the time goes in v1:
time: 120 us; the launch traced here: 119 us
  blocking collectives  35.4 us (30%)
  waiting for transfers between devices  29.3 us (24%)
  starting transfers between devices  15.3 us (13%)
  between operations  14.4 us (12%)
  local copies, waits for them, and re-layouts  9.87 us (8%)
  other arithmetic  8.29 us (7%)
  matrix products  6.87 us (6%)
    reduce_scatter x1, waiting for transfers between devices, shards(): lax.psum_scatter(partial_value.astype(jnp.bfloat16), 'tp', scatter_dimens...  16.4 us
    all_to_all x1, blocking collectives, shards(): lax.all_to_all(buffer.reshape(experts_all, capacity, own_cols.shape[1]),...  12.8 us
    all_to_all x1, waiting for transfers between devices, shards(): lax.all_to_all(reduced, 'ep', split_axis=1, concat_axis=0, tiled=True)  6.2 us
    all_gather x1, blocking collectives, shards(): lax.all_gather(q_part, 'tp', axis=1, tiled=True)  6.14 us
    all_gather x1, blocking collectives, shards(): piece = lax.all_gather(arrived, 'tp', axis=2, tiled=True)  5.6 us
    all_to_all x1, starting transfers between devices, shards(): lax.all_to_all(reduced, 'ep', split_axis=1, concat_axis=0, tiled=True)  5.52 us
    all_gather x1, blocking collectives, shards(): lax.all_gather(kv_part, 'tp', axis=1, tiled=True)  5.42 us
    all_gather x1, blocking collectives, shards(): lax.all_gather(jnp.dot(head_values, attn_out, preferred_element_type=jnp....  5.41 us
  transfers between devices with their start and end apart: 5, of which 4 were waited for; matrix products, arithmetic and copies ran while one was open for 8% of the time, Pallas kernels for 0%

profile of v1, /device:TPU:0, one launch (start us, length us, event | category | flops | bytes accessed | tf_op | source)
XLA Modules:
  0.0 119.5 jit_solution(2239073504966215824)
XLA Ops:
  7.2 1.0 fusion.19
  8.3 1.2 convolution_convert_fusion.6
  9.5 6.1 %all_gather.15 = bf16[16,512]{1,0:T(8,128)(2,1)S(1)} all-gather(bf16[16,128]{1,0:T(8,128)(2,1)S(1)} %convolution_convert_fusion.6), channel_id=1, replica_groups=mesh['ep'=8,'tp'=4] {'tp'}, dimensions={1}, use_global_device_ids=true | all-gather | bytes 20480 | tf_op jit(solution)/shard_map/all_gather | solution.py:83
  15.7 1.1 fusion.42
  17.1 0.7 convert_element_type.134
  17.8 0.8 fusion.46
  18.9 0.7 reshape.331
  19.5 3.3 %all-to-all-start.1 = ((bf16[4,2,128]{2,1,0:T(2,128)(2,1)}), bf16[4,2,128]{2,1,0:T(2,128)(2,1)S(1)}, u32[]{:S(2)}, u32[]{:S(2)}) async-start(bf16[4,2,128]{2,1,0:T(2,128)(2,1)} %reshape.331), calls=%async_computation.1 | async-start | bytes 4096 | tf_op jit(solution)/shard_map/all_to_all | solution.py:109
  22.8 0.7 broadcast_multiply_fusion
  23.5 0.8 copy.100
  24.3 0.2 convert_reduce_fusion
  24.5 1.0 copy.90
  25.7 0.9 convert_element_type.135
  26.6 0.2 multiply_cosine_fusion
  26.8 0.7 fusion.71
  27.6 1.2 convolution_convert_fusion.5
  28.8 5.4 %all_gather.16 = bf16[16,512]{1,0:T(8,128)(2,1)S(1)} all-gather(bf16[16,128]{1,0:T(8,128)(2,1)S(1)} %convolution_convert_fusion.5), channel_id=1, replica_groups=mesh['ep'=8,'tp'=4] {'tp'}, dimensions={1}, use_global_device_ids=true | all-gather | bytes 20480 | tf_op jit(solution)/shard_map/all_gather | solution.py:84
  34.5 0.2 convolution_convert_fusion.4
  35.1 0.6 copy.91
  35.7 3.3 %all-to-all-start = ((bf16[16,2,512]{2,1,0:T(2,128)(2,1)}), bf16[16,2,512]{2,1,0:T(2,128)(2,1)S(1)}, u32[]{:S(2)}, u32[]{:S(2)}) async-start(bf16[16,2,512]{2,1,0:T(2,128)(2,1)} %copy.91), calls=%async_computation | async-start | bytes 65536 | tf_op jit(solution)/shard_map/all_to_all | solution.py:108
  39.2 3.7 %all-to-all-done = bf16[16,2,512]{2,1,0:T(2,128)(2,1)S(1)} async-done(((bf16[16,2,512]{2,1,0:T(2,128)(2,1)}), bf16[16,2,512]{2,1,0:T(2,128)(2,1)S(1)}, u32[]{:S(2)}, u32[]{:S(2)}) %all-to-all-start) | async-done | bytes 32800 | tf_op jit(solution)/shard_map/all_to_all | solution.py:108
  43.0 0.6 fusion.73
  43.6 0.1 fusion.49
  43.8 0.2 fusion.72
  44.0 0.2 fusion.23
  44.2 0.4 fusion.4
  44.7 0.6 copy.95
  45.3 3.3 %all-to-all-start.2 = ((bf16[4,8,512]{2,0,1:T(4,128)(2,1)}), bf16[4,8,512]{2,0,1:T(4,128)(2,1)S(1)}, u32[]{:S(2)}, u32[]{:S(2)}) async-start(bf16[4,8,512]{2,0,1:T(4,128)(2,1)} %copy.95), calls=%async_computation.2 | async-start | bytes 65536 | tf_op jit(solution)/shard_map/all_to_all | solution.py:146
  48.7 0.8 dynamic-slice
  49.5 2.9 %all-to-all-done.2 = bf16[4,8,512]{2,0,1:T(4,128)(2,1)S(1)} async-done(((bf16[4,8,512]{2,0,1:T(4,128)(2,1)}), bf16[4,8,512]{2,0,1:T(4,128)(2,1)S(1)}, u32[]{:S(2)}, u32[]{:S(2)}) %all-to-all-start.2) | async-done | bytes 32800 | tf_op jit(solution)/shard_map/all_to_all | solution.py:146
  52.5 0.1 fusion.7
  52.8 0.1 convolution_convert_fusion.1
  52.9 5.4 %all-gather = bf16[64,1024]{1,0:T(8,128)(2,1)S(1)} all-gather(bf16[16,1024]{1,0:T(8,128)(2,1)S(1)} %convolution_convert_fusion.1), channel_id=2, replica_groups=mesh['ep'=8,'tp'=4] {'tp'}, dimensions={0}, use_global_device_ids=true | all-gather | bytes 163840 | tf_op jit(solution)/shard_map/all_gather | solution.py:158
  58.6 0.9 scatter_custom_fusion
  59.6 12.8 %all_to_all.75 = bf16[8,12,256]{2,1,0:T(8,128)(2,1)S(1)} all-to-all(bf16[8,12,256]{2,1,0:T(8,128)(2,1)S(1)} %reshape.301), channel_id=1, replica_groups=mesh['ep'=8,'tp'=4] {'ep'}, dimensions={0} | all-to-all | bytes 98304 | tf_op jit(solution)/shard_map/all_to_all | solution.py:183
  72.4 5.6 %all_gather.19 = bf16[1,96,1024]{2,1,0:T(8,128)(2,1)S(1)} all-gather(bf16[1,96,256]{2,1,0:T(8,128)(2,1)S(1)} %all_to_all.68), channel_id=1, replica_groups=mesh['ep'=8,'tp'=4] {'tp'}, dimensions={2}, use_global_device_ids=true | all-gather | bytes 245760 | tf_op jit(solution)/shard_map/all_gather | solution.py:190
  78.0 0.2 fusion.11
  78.2 1.0 fusion
  79.4 16.4 %reduce-scatter.2.cloned.1.call-done = bf16[1,96,256]{2,1,0:T(8,128)(2,1)} async-done(((bf16[1,96,1024]{2,1,0:T(8,128)(2,1)}), bf16[1,96,256]{2,1,0:T(8,128)(2,1)}) %reduce-scatter.2.cloned.1.call-update) | async-done | bytes 49168 | tf_op jit(solution)/shard_map/reduce_scatter | solution.py:197
  95.8 0.9 copy.122
  96.7 0.5 broadcast.235
  97.2 0.9 reduce.1
  98.1 0.6 reshape.333
  98.7 5.5 %all-to-all-start.4 = ((bf16[8,2,1536]{2,1,0:T(2,128)(2,1)}), bf16[8,2,1536]{2,1,0:T(2,128)(2,1)S(1)}, u32[]{:S(2)}, u32[]{:S(2)}) async-start(bf16[8,2,1536]{2,1,0:T(2,128)(2,1)} %reshape.333), calls=%async_computation.5 | async-start | bytes 98304 | tf_op jit(solution)/shard_map/all_to_all | solution.py:200
  104.3 0.6 constant_dynamic-slice_fusion
  104.9 6.2 %all-to-all-done.4 = bf16[8,2,1536]{2,1,0:T(2,128)(2,1)S(1)} async-done(((bf16[8,2,1536]{2,1,0:T(2,128)(2,1)}), bf16[8,2,1536]{2,1,0:T(2,128)(2,1)S(1)}, u32[]{:S(2)}, u32[]{:S(2)}) %all-to-all-start.4) | async-done | bytes 49184 | tf_op jit(solution)/shard_map/all_to_all | solution.py:200
  111.1 0.8 gather_fusion
  112.0 0.6 add_convert_fusion.1
  (81 shorter events, 2.8 us)
Async XLA Ops:
  7.2 35.8 %copy-start = (bf16[4,512,512]{2,1,0:T(8,128)(2,1)S(1)}, bf16[4,512,512]{2,1,0:T(8,128)(2,1)}, u32[]{:S(2)}) copy-start(bf16[4,512,512]{2,1,0:T(8,128)(2,1)} %param.33) | copy-start | bytes 6291460
  7.2 27.3 %copy-start.5 = (bf16[16,1024]{1,0:T(8,128)(2,1)S(1)}, bf16[16,1024]{1,0:T(8,128)(2,1)}, u32[]{:S(2)}) copy-start(bf16[16,1024]{1,0:T(8,128)(2,1)} %param.21) | copy-start | bytes 98308
  7.2 27.3 %copy-start.11 = (f32[1024]{0:T(1024)S(1)}, f32[1024]{0:T(1024)}, u32[]{:S(2)}) copy-start(f32[1024]{0:T(1024)} %param.22) | copy-start | bytes 12292
  7.2 27.1 %copy-start.8 = (f32[512]{0:T(512)S(1)}, f32[512]{0:T(512)}, u32[]{:S(2)}) copy-start(f32[512]{0:T(512)} %param.27) | copy-start | bytes 6148
  7.2 27.2 %copy-start.10 = (bf16[1024,32]{0,1:T(8,128)(2,1)S(1)}, bf16[1024,32]{0,1:T(8,128)(2,1)}, u32[]{:S(2)}) copy-start(bf16[1024,32]{0,1:T(8,128)(2,1)} %param.25) | copy-start | bytes 196612
  19.5 16.2 %all-to-all-start.1 = ((bf16[4,2,128]{2,1,0:T(2,128)(2,1)}), bf16[4,2,128]{2,1,0:T(2,128)(2,1)S(1)}, u32[]{:S(2)}, u32[]{:S(2)}) async-start(bf16[4,2,128]{2,1,0:T(2,128)(2,1)} %reshape.331), calls=%async_computation.1 | async-start | bytes 4096 | tf_op jit(solution)/shard_map/all_to_all | solution.py:109
  34.7 10.0 %copy-start.9 = (bf16[16,32]{1,0:T(8,128)(2,1)}, bf16[16,32]{1,0:T(8,128)(2,1)S(1)}, u32[]{:S(2)}) copy-start(bf16[16,32]{1,0:T(8,128)(2,1)S(1)} %convolution_convert_fusion.4) | copy-start | bytes 3076
  35.7 7.2 %all-to-all-start = ((bf16[16,2,512]{2,1,0:T(2,128)(2,1)}), bf16[16,2,512]{2,1,0:T(2,128)(2,1)S(1)}, u32[]{:S(2)}, u32[]{:S(2)}) async-start(bf16[16,2,512]{2,1,0:T(2,128)(2,1)} %copy.91), calls=%async_computation | async-start | bytes 65536 | tf_op jit(solution)/shard_map/all_to_all | solution.py:108
  43.0 5.6 %copy-start.6 = (bf16[512,128]{1,0:T(8,128)(2,1)S(1)}, bf16[512,128]{1,0:T(8,128)(2,1)}, u32[]{:S(2)}) copy-start(bf16[512,128]{1,0:T(8,128)(2,1)} %param.31) | copy-start | bytes 393220
  43.6 9.1 %copy-start.1 = (bf16[128,1024]{1,0:T(8,128)(2,1)S(1)}, bf16[128,1024]{1,0:T(8,128)(2,1)}, u32[]{:S(2)}) copy-start(bf16[128,1024]{1,0:T(8,128)(2,1)} %param.32) | copy-start | bytes 786436
  44.2 33.8 %copy-start.2 = (bf16[1,1024,128]{2,1,0:T(8,128)(2,1)S(1)}, bf16[1,1024,128]{2,1,0:T(8,128)(2,1)}, u32[]{:S(2)}) copy-start(bf16[1,1024,128]{2,1,0:T(8,128)(2,1)} %param.39) | copy-start | bytes 786436
  44.2 34.0 %copy-start.3 = (bf16[1,128,1024]{2,1,0:T(8,128)(2,1)S(1)}, bf16[1,128,1024]{2,1,0:T(8,128)(2,1)}, u32[]{:S(2)}) copy-start(bf16[1,128,1024]{2,1,0:T(8,128)(2,1)} %param.41) | copy-start | bytes 786436
  44.2 34.0 %copy-start.4 = (bf16[1,1024,128]{2,1,0:T(8,128)(2,1)S(1)}, bf16[1,1024,128]{2,1,0:T(8,128)(2,1)}, u32[]{:S(2)}) copy-start(bf16[1,1024,128]{2,1,0:T(8,128)(2,1)} %param.40) | copy-start | bytes 786436
  44.7 34.6 %copy-start.7 = (f32[16,6]{0,1:T(8,128)S(1)}, f32[16,6]{0,1:T(8,128)}, u32[]{:S(2)}) copy-start(f32[16,6]{0,1:T(8,128)} %param.38) | copy-start | bytes 1156
  45.3 7.2 %all-to-all-start.2 = ((bf16[4,8,512]{2,0,1:T(4,128)(2,1)}), bf16[4,8,512]{2,0,1:T(4,128)(2,1)S(1)}, u32[]{:S(2)}, u32[]{:S(2)}) async-start(bf16[4,8,512]{2,0,1:T(4,128)(2,1)} %copy.95), calls=%async_computation.2 | async-start | bytes 65536 | tf_op jit(solution)/shard_map/all_to_all | solution.py:146
  48.6 47.2 %reduce-scatter.2.cloned.1.call-start = ((), (), s32[]{:S(2)}) async-start(), calls=%async_computation.6 | async-start | bytes 245760 | tf_op jit(solution)/shard_map/reduce_scatter | solution.py:197
  98.7 12.3 %all-to-all-start.4 = ((bf16[8,2,1536]{2,1,0:T(2,128)(2,1)}), bf16[8,2,1536]{2,1,0:T(2,128)(2,1)S(1)}, u32[]{:S(2)}, u32[]{:S(2)}) async-start(bf16[8,2,1536]{2,1,0:T(2,128)(2,1)} %reshape.333), calls=%async_computation.5 | async-start | bytes 98304 | tf_op jit(solution)/shard_map/all_to_all | solution.py:200
Sparse Core Ops, SparseCore 0:
  79.4 16.3 reduce-scatter.1
